TPU v7x, 128 devices: a whole 4x4x4 slice. The times are simulated.
128 devices in a mesh: ep: 128 (over z, y, x, core).
Axes of the slice: x: 4, y: 4, z: 4, core: 2. Of those that a mesh axis runs over, the one named last changes fastest.
Arguments:
- tokens: bfloat16 [2304, 2048], P('ep'), may hold values from -6 to 6
- attn_norm_gain: float32 [2048], replicated, may hold values from 0.1 to 1.9
- w_query: bfloat16 [2048, 512], replicated, may hold values from -0.125 to 0.125
- w_key: bfloat16 [2048, 128], replicated, may hold values from -0.125 to 0.125
- w_value: bfloat16 [2048, 128], replicated, may hold values from -0.125 to 0.125
- w_forget: bfloat16 [2048, 8], replicated, may hold values from -0.125 to 0.125
- forget_bias: float32 [8], replicated, may hold values from 0.5 to 4
- w_attn_out: bfloat16 [512, 2048], replicated, may hold values from -0.25 to 0.25
- cache_keys: bfloat16 [2304, 1024, 128], P('ep'), may hold values from -72 to 72
- cache_values: bfloat16 [2304, 1024, 128], P('ep'), may hold values from -6 to 6
- cache_logcum: float32 [2304, 8, 1024], P('ep'), as said below
- cache_lengths: int32 [2304], P('ep'), may hold values from 128 to 1024
- expert_norm_gain: float32 [2048], replicated, may hold values from 0.4 to 40
- expert_ids: int32 [2304, 6], P('ep'), may hold values from 0 to 127, all different within a row; in each aligned block of 18 rows (0 to 17, 18 to 35, ...) at most 2 rows name the same one
- expert_weights: float32 [2304, 6], P('ep'), may hold values from 0.1 to 1
- w_expert_gate: bfloat16 [128, 2048, 512], P('ep'), may hold values from -0.125 to 0.125
- w_expert_up: bfloat16 [128, 2048, 512], P('ep'), may hold values from -0.125 to 0.125
- w_expert_down: bfloat16 [128, 512, 2048], P('ep'), may hold values from -0.25 to 0.25
- w_dense_gate: bfloat16 [2048, 4096], P(None, 'ep'), may hold values from -0.125 to 0.125
- w_dense_up: bfloat16 [2048, 4096], P(None, 'ep'), may hold values from -2 to 2
- w_dense_down: bfloat16 [4096, 2048], P('ep'), may hold values from -0.09375 to 0.09375
- dense_norm_gain: float32 [4096], replicated, may hold values from 0.1 to 1.9
- branch_gate: float32 [2048], replicated, may hold values from -0.125 to 0.125
Outputs:
- result: bfloat16 [2304, 2048], P('ep')
Inputs may be any that keep to these rules, and one draw needn't show every extreme that they name: `cache_logcum`: along the positions of each sequence and head the values never rise. `expert_ids`: each row names 6 different experts; among the rows of one device no expert is named by more than 2 rows, and in every draw some device names some expert exactly 2 times.
All inputs are finite; a program needn't handle non-finite values.
Results may differ from a plain program's by a relative error of at most 0.012.
The roundings to bfloat16 on the way count: a program that leaves them out, or rounds other values in their place, can miss the bound.
Values may be sent and summed in bfloat16 or wider, within the bound.
No kernel may reach another device: no remote copies, remote signals or barrier semaphores. Data moves between devices by JAX's collectives and lax.ppermute only.
A program may use at most 128 MiB of HBM per device.

v0:
```python
import jax
import jax.numpy as jnp
from jax import lax
from jax.experimental import pallas as pl
from jax.experimental.pallas import tpu as pltpu
from jax.sharding import PartitionSpec as P


HEADS = 8
KV_HEADS = 2
HEAD_DIM = 64
TOPK = 6
EPS = 1e-06
LIMIT = 7.0
ALPHA = 1.702
CAP = 2
PLANE = 32
CORES = 2
PARTS = 8
DENSE_FF = 4096
F32 = jnp.float32
BF16 = jnp.bfloat16
VMEM = pl.BlockSpec(memory_space=pltpu.VMEM)
HBM = pl.BlockSpec(memory_space=pltpu.HBM)
NT = (((1,), (1,)), ((), ()))
TN = (((0,), (0,)), ((), ()))


def dot(a, b):
    return jnp.dot(a, b, preferred_element_type=F32)


def slot_masks(slots, seqs):
    slot = lax.broadcasted_iota(jnp.int32, (slots, seqs), 0)
    token = lax.broadcasted_iota(jnp.int32, (slots, seqs), 1)
    device = slot // CAP
    part = (device // PLANE) * CORES + device % CORES
    dense = token == part + PARTS * (slot % CAP)
    extra = token == part + PARTS * CAP
    return slot, device, dense, extra


def fill_outgoing(
    routed_in, ids_ref, eweights_ref, place_ref, outgoing_ref, outgoing_hbm, out_sems
):
    seqs, width = routed_in.shape
    half = width // CAP
    slots = outgoing_ref.shape[0] * CAP
    slot, device, dense, extra = slot_masks(slots, seqs)
    member = jnp.zeros((slots, seqs), F32)
    share = jnp.zeros((slots, seqs), F32)
    for k in range(TOPK):
        hit = ids_ref[k:k + 1, :] == device
        member = member + jnp.where(hit, 1.0, 0.0)
        share = share + jnp.where(hit, eweights_ref[k:k + 1, :], 0.0)
    earlier = lax.broadcasted_iota(jnp.int32, (seqs, seqs), 0)
    later = lax.broadcasted_iota(jnp.int32, (seqs, seqs), 1)
    before = jnp.where(earlier < later, 1.0, 0.0).astype(BF16)
    prior = dot(member.astype(BF16), before)
    here = prior == (slot % CAP).astype(F32)
    place_ref[...] = jnp.where(here, share, 0.0)
    routes = jnp.where(here, member, 0.0).astype(BF16)
    extra = jnp.where(extra, 1.0, 0.0).astype(BF16)
    even = lax.broadcasted_iota(jnp.int32, (slots, half), 0) % CAP == 0
    third = jnp.where(even, dot(extra, routed_in[:, :half]), dot(extra, routed_in[:, half:]))
    devices = slots // CAP
    copies = []

    def send(start, stop, value):
        window = (slice(None), slice(None), pl.ds(start, stop - start))
        outgoing_ref[window] = value.astype(BF16).reshape(devices, CAP, stop - start)
        copies.append(pltpu.make_async_copy(
            outgoing_ref.at[window], outgoing_hbm.at[window], out_sems.at[len(copies)]))
        copies[-1].start()

    send(2 * width, 2 * width + half, third)
    send(width, 2 * width, dot(jnp.where(dense, 1.0, 0.0).astype(BF16), routed_in))
    send(0, width, dot(routes, routed_in))
    for copy in copies:
        copy.wait()


def mixer_body(
    tokens_hbm, again_hbm, wq_hbm, wk_hbm, wv_hbm, wf_hbm, fbias_hbm, wo_hbm,
    keys_hbm, values_hbm, logcum_hbm, lengths_hbm, egain_hbm, bgate_hbm, ids_hbm, eweights_hbm,
    mixed_ref, branch_ref, place_ref, outgoing_hbm,
    tokens_ref, again_ref, wq, wk, wv, wf_ref, fbias_ref, wo,
    kbuf, vbuf, cbuf, lengths_ref, egain_ref, bgate_ref, ids_ref, eweights_ref, sems,
    outgoing_ref, out_sems,
):
    sources = dict(
        tokens=(tokens_hbm, tokens_ref), again=(again_hbm, again_ref), wf=(wf_hbm, wf_ref),
        fbias=(fbias_hbm, fbias_ref), lengths=(lengths_hbm, lengths_ref), wq=(wq_hbm, wq),
        wk=(wk_hbm, wk), wv=(wv_hbm, wv), keys=(keys_hbm, kbuf), logcum=(logcum_hbm, cbuf),
        values=(values_hbm, vbuf), wo=(wo_hbm, wo), egain=(egain_hbm, egain_ref),
        bgate=(bgate_hbm, bgate_ref), ids=(ids_hbm, ids_ref), eweights=(eweights_hbm, eweights_ref))
    copies = {}
    for i, (name, (source, target)) in enumerate(sources.items()):
        copies[name] = pltpu.make_async_copy(source, target, sems.at[i])
        copies[name].start()

    def ready(*names):
        for name in names:
            copies[name].wait()

    seqs, _ = tokens_ref.shape
    length = kbuf.shape[1]
    rows = seqs * HEADS
    ready("tokens", "again", "wf", "fbias", "lengths")
    x = tokens_ref[...].astype(F32)
    scale = lax.rsqrt(jnp.mean(x * x, axis=1, keepdims=True) + EPS)
    normed = (x * scale * again_ref[...]).astype(BF16)
    forget = lax.dot_general(normed, wf_ref[...], NT, preferred_element_type=F32) + fbias_ref[...]
    log_forget = jax.nn.log_sigmoid(forget)
    row = lax.broadcasted_iota(jnp.int32, (rows, seqs), 0)
    col = lax.broadcasted_iota(jnp.int32, (rows, seqs), 1)
    spread_mask = (row // HEADS) == col
    spread = jnp.where(spread_mask, 1.0, 0.0).astype(BF16)
    live_len = jnp.sum(jnp.where(spread_mask, lengths_ref[...], 0), axis=1, keepdims=True)
    head8 = lax.broadcasted_iota(jnp.int32, (rows, HEADS), 0) % HEADS
    lane8 = lax.broadcasted_iota(jnp.int32, (rows, HEADS), 1)
    lf_rows = lax.dot_general(
        jnp.where(spread_mask, 1.0, 0.0), log_forget, (((1,), (0,)), ((), ())),
        precision=lax.Precision.HIGHEST, preferred_element_type=F32)
    lf_rows = jnp.sum(jnp.where(head8 == lane8, lf_rows, 0.0), axis=1, keepdims=True)

    ready("wq", "wk", "wv")
    query = dot(normed, wq[...]).astype(BF16)
    key_new = dot(normed, wk[...]).astype(BF16)
    value_new = dot(normed, wv[...]).astype(BF16)
    q_rows = dot(spread, query)
    key_rows = dot(spread, key_new)
    value_rows = dot(spread, value_new)
    head = lax.broadcasted_iota(jnp.int32, (rows, 128), 0) % HEADS
    lane = lax.broadcasted_iota(jnp.int32, (rows, 128), 1)
    half = lane // HEAD_DIM
    kv_half = head // (HEADS // KV_HEADS)
    q_sel = jnp.zeros((rows, 128), F32)
    for b in range(HEADS // 2):
        block = q_rows[:, 128 * b:128 * b + 128]
        turned = pltpu.roll(block, HEAD_DIM, 1)
        q_sel = jnp.where(head // 2 == b, jnp.where(head % 2 == kv_half, block, turned), q_sel)
    q_sel = jnp.where(half == kv_half, q_sel, 0.0)
    own = jnp.sum(q_sel * key_rows, axis=1, keepdims=True) * (HEAD_DIM ** -0.5)
    q_bf = q_sel.astype(BF16)
    seq_row = lax.broadcasted_iota(jnp.int32, (rows, 128), 0) // HEADS
    blocks = [jnp.where(seq_row == s, q_sel, 0.0).astype(BF16) for s in range(seqs)]
    q_block = jnp.concatenate(blocks, axis=1)

    ready("keys")
    k_all = jnp.concatenate([kbuf[s] for s in range(seqs)], axis=1)
    scores_t = lax.dot_general(k_all, q_block, NT, preferred_element_type=F32)
    scores = jnp.transpose(scores_t)
    ready("logcum")
    logcum = cbuf[...].reshape(rows, length)
    place = lax.broadcasted_iota(jnp.int32, (rows, length), 1)
    last = jnp.sum(jnp.where(place == live_len - 1, logcum, 0.0), axis=1, keepdims=True)
    carried = last + lf_rows
    scores = scores * (HEAD_DIM ** -0.5) + (carried - logcum)
    scores = jnp.where(place < live_len, scores, -jnp.inf)
    top = jnp.maximum(jnp.max(scores, axis=1, keepdims=True), own)
    expo = jnp.exp(scores - top)
    own_expo = jnp.exp(own - top)
    total = jnp.sum(expo, axis=1, keepdims=True) + own_expo
    weights = (expo / total).astype(BF16)
    own_weight = (own_expo / total).astype(BF16).astype(F32)

    ready("values")
    parts = []
    for p in range(seqs // 2):
        v_pair = jnp.concatenate([vbuf[2 * p], vbuf[2 * p + 1]], axis=1)
        both = dot(weights[16 * p:16 * p + 16], v_pair)
        parts.append(both[:8, :128])
        parts.append(both[8:, 128:])
    out = jnp.concatenate(parts, axis=0) + own_weight * value_rows
    out = jnp.where(half == kv_half, out, 0.0)
    out_turned = pltpu.roll(out, HEAD_DIM, 1)
    outs = []
    for b in range(HEADS // 2):
        piece = jnp.where(head // 2 == b, jnp.where(head % 2 == kv_half, out, out_turned), 0.0)
        outs.append(lax.dot_general(spread, piece.astype(BF16), TN, preferred_element_type=F32))
    attended = jnp.concatenate(outs, axis=1).astype(BF16)
    ready("wo", "egain", "bgate", "ids", "eweights")
    mixed = (x + dot(attended, wo[...])).astype(BF16)
    mixed_ref[...] = mixed
    y = mixed.astype(F32)
    scale = lax.rsqrt(jnp.mean(y * y, axis=1, keepdims=True) + EPS)
    routed_in = (y * scale * egain_ref[...]).astype(BF16)
    branch = jax.nn.sigmoid(jnp.sum(routed_in.astype(F32) * bgate_ref[...], axis=1, keepdims=True))
    branch_ref[...] = jnp.broadcast_to(branch, branch_ref.shape)
    fill_outgoing(
        routed_in, ids_ref, eweights_ref, place_ref, outgoing_ref, outgoing_hbm, out_sems)


def mixer(tokens, attn_norm_gain, w_query, w_key, w_value, w_forget, forget_bias, w_attn_out,
          cache_keys, cache_values, cache_logcum, cache_lengths, expert_norm_gain, branch_gate,
          expert_ids, expert_weights, devices):
    seqs, width = tokens.shape
    operands = (
        tokens, attn_norm_gain.reshape(1, width), w_query, w_key, w_value, w_forget.T,
        forget_bias.reshape(1, HEADS), w_attn_out, cache_keys, cache_values, cache_logcum,
        cache_lengths.reshape(1, seqs), expert_norm_gain.reshape(1, width),
        branch_gate.reshape(1, width), expert_ids.T, expert_weights.T)
    operands = tuple(pltpu.with_memory_space_constraint(a, pltpu.HBM) for a in operands)
    return pl.pallas_call(
        mixer_body,
        out_shape=(
            jax.ShapeDtypeStruct((seqs, width), BF16),
            jax.ShapeDtypeStruct((seqs, 128), F32),
            jax.ShapeDtypeStruct((devices * CAP, seqs), F32),
            pltpu.HBM((devices, CAP, 2 * width + width // CAP), BF16),
        ),
        in_specs=[HBM] * len(operands),
        out_specs=(VMEM, VMEM, VMEM, HBM),
        scratch_shapes=[pltpu.VMEM(a.shape, a.dtype) for a in operands]
        + [
            pltpu.SemaphoreType.DMA((len(operands),)),
            pltpu.VMEM((devices, CAP, 2 * width + width // CAP), BF16),
            pltpu.SemaphoreType.DMA((3,)),
        ],
        compiler_params=pltpu.CompilerParams(vmem_limit_bytes=28 * 1024 * 1024),
        cost_estimate=pl.CostEstimate(flops=10**10, bytes_accessed=15 * 2**20, transcendentals=0),
        name="mixer",
    )(*operands)


def pair(a):
    return a.reshape(a.shape[0] // CAP, CAP, a.shape[1])


def worker_body(
    device_ref, arrived_ref, gate_hbm, up_hbm, down_hbm,
    h0, h1, h2, h3, h4, h5, h6, h7, gain_ref,
    answer_ref, wg, wu, wd, held, sems,
):
    devices, cap, _ = arrived_ref.shape
    rows = devices * cap
    width = wd.shape[1]
    half = width // CAP
    weight_copies = [
        pltpu.make_async_copy(source.at[0], target, sems.at[i])
        for i, (source, target) in enumerate(((gate_hbm, wg), (up_hbm, wu), (down_hbm, wd)))]
    piece_copies = [
        pltpu.make_async_copy(source, held.at[i], sems.at[3 + i])
        for i, source in enumerate((h0, h1, h2, h3, h4, h5, h6, h7))]
    for copy in weight_copies + piece_copies:
        copy.start()
    x = arrived_ref[:, :, :width].reshape(rows, width)
    weight_copies[0].wait()
    gate = jnp.minimum(dot(x, wg[...]), LIMIT)
    weight_copies[1].wait()
    up = jnp.clip(dot(x, wu[...]), -LIMIT, LIMIT)
    act = ((up + 1.0) * gate * jax.nn.sigmoid(gate * ALPHA)).astype(BF16)
    weight_copies[2].wait()
    answer_ref[:, :, :width] = pair(dot(act, wd[...]).astype(BF16))

    units = held.shape[1] // 3
    me = device_ref[0]
    gains = []
    lane = lax.broadcasted_iota(jnp.int32, (1, 128), 1)
    per_row = 128 // units
    for block in range(PARTS // per_row):
        vec = jnp.zeros((1, 128), F32)
        for q in range(per_row):
            p = block * per_row + q
            owner = lax.rem(me + (PARTS // CORES - p // CORES) * PLANE, devices)
            if p % CORES:
                owner = owner + 1 - 2 * lax.rem(me, CORES)
            line = gain_ref[pl.ds(owner // per_row, 1), :]
            shift = lax.rem(q - lax.rem(owner, per_row) + per_row, per_row) * units
            vec = jnp.where(lane // units == q, pltpu.roll(line, shift, 1), vec)
        gains.append(vec)
    gain = jnp.concatenate(gains, axis=1)
    for copy in piece_copies:
        copy.wait()
    dg = jnp.concatenate([held[p, :units] for p in range(PARTS)], axis=0)
    du = jnp.concatenate([held[p, units:2 * units] for p in range(PARTS)], axis=0)
    dd = jnp.concatenate([held[p, 2 * units:] for p in range(PARTS)], axis=0)

    def nt(a, b):
        return lax.dot_general(a, b, NT, preferred_element_type=F32)

    def hidden_of(gate, up):
        kept = (jax.nn.silu(gate) * up).astype(BF16).astype(F32)
        square = jnp.sum(kept * kept, axis=1, keepdims=True)
        return (kept * gain).astype(BF16), square

    first = arrived_ref[:, :, width:2 * width].reshape(rows, width)
    extra = arrived_ref[:, :, 2 * width:].reshape(rows, half)
    hid, square = hidden_of(nt(first, dg), nt(first, du))
    answer_ref[:, :, width:2 * width] = pair(dot(hid, dd).astype(BF16))
    even = lax.broadcasted_iota(jnp.int32, (rows, PARTS * units), 0) % CAP == 0

    def joined(weight):
        both = jnp.where(even, nt(extra, weight[:, :half]), nt(extra, weight[:, half:]))
        return both + pltpu.roll(both, rows - 1, 0)

    hid3, square3 = hidden_of(joined(dg), joined(du))
    low = dot(hid3, dd[:, :half])
    high = pltpu.roll(dot(hid3, dd[:, half:]), 1, 0)
    even = lax.broadcasted_iota(jnp.int32, (rows, half), 0) % CAP == 0
    answer_ref[:, :, 2 * width:2 * width + half] = pair(jnp.where(even, low, high).astype(BF16))
    lane = lax.broadcasted_iota(jnp.int32, (rows, 128), 1)
    head = jnp.where(lane < 2, square, square3)
    top = head.astype(BF16).astype(F32)
    tail = jnp.where(lane % 2 == 0, top, head - top)
    answer_ref[:, :, 2 * width + half:] = pair(jnp.where(lane < 4, tail, 0.0).astype(BF16))


def worker(device, arrived, gate_w, up_w, down_w, pieces, gain):
    devices, cap, packed = arrived.shape
    stored = tuple(
        pltpu.with_memory_space_constraint(a, pltpu.HBM) for a in (gate_w, up_w, down_w))
    pieces = tuple(pltpu.with_memory_space_constraint(a, pltpu.HBM) for a in pieces)
    return pl.pallas_call(
        worker_body,
        out_shape=jax.ShapeDtypeStruct((devices, cap, packed + 128), BF16),
        in_specs=[pl.BlockSpec(memory_space=pltpu.SMEM), VMEM] + [HBM] * 11 + [VMEM],
        out_specs=VMEM,
        scratch_shapes=[pltpu.VMEM(a.shape[1:], BF16) for a in stored]
        + [
            pltpu.VMEM((len(pieces),) + pieces[0].shape, BF16),
            pltpu.SemaphoreType.DMA((3 + len(pieces),)),
        ],
        compiler_params=pltpu.CompilerParams(vmem_limit_bytes=28 * 1024 * 1024),
        cost_estimate=pl.CostEstimate(flops=5 * 10**9, bytes_accessed=15 * 2**20, transcendentals=0),
        name="worker",
    )(device, arrived, *stored, *pieces, gain.reshape(-1, 128))


def merger_body(returned_ref, place_ref, mixed_ref, branch_ref, result_ref):
    devices, cap, _ = returned_ref.shape
    seqs, width = mixed_ref.shape
    rows = devices * cap
    half = width // CAP

    def tn(a, b):
        return lax.dot_general(a, b, TN, preferred_element_type=F32)

    slot, _, dense, extra = slot_masks(rows, seqs)
    share = place_ref[...]
    s1 = share.astype(BF16)
    rest = share - s1.astype(F32)
    s2 = rest.astype(BF16)
    s3 = (rest - s2.astype(F32)).astype(BF16)
    answers = returned_ref[:, :, :width].reshape(rows, width)
    routed = tn(s1, answers) + tn(s2, answers) + tn(s3, answers)
    dense = jnp.where(dense, 1.0, 0.0).astype(BF16)
    low = jnp.where(extra & (slot % CAP == 0), 1.0, 0.0).astype(BF16)
    high = jnp.where(extra & (slot % CAP == 1), 1.0, 0.0).astype(BF16)
    total = tn(dense, returned_ref[:, :, width:2 * width].reshape(rows, width))
    third = returned_ref[:, :, 2 * width:2 * width + half].reshape(rows, half)
    total = total + jnp.concatenate([tn(low, third), tn(high, third)], axis=1)
    sums = returned_ref[:, :, 2 * width + half:].reshape(rows, 128)
    lane = lax.broadcasted_iota(jnp.int32, (seqs, 128), 1)
    square = jnp.where(lane < 2, tn(dense, sums), 0.0)
    square = square + jnp.where((lane >= 2) & (lane < 4), tn(low, sums), 0.0)
    square = jnp.sum(square, axis=1, keepdims=True)
    unit_scale = lax.rsqrt(square / DENSE_FF + EPS)
    out = mixed_ref[...].astype(F32) + routed + branch_ref[:, :1] * (total * unit_scale)
    result_ref[...] = out.astype(BF16)


def merger(returned, place, mixed, branch):
    return pl.pallas_call(
        merger_body,
        out_shape=jax.ShapeDtypeStruct(mixed.shape, BF16),
        in_specs=[VMEM] * 4,
        out_specs=VMEM,
        compiler_params=pltpu.CompilerParams(vmem_limit_bytes=16 * 1024 * 1024),
        name="merger",
    )(returned, place, mixed, branch)


def gather_pieces(own, devices):
    def moved(array, target):
        return lax.ppermute(array, "ep", [(d, target(d)) for d in range(devices)])

    pieces = []
    for hop in range(PARTS // CORES):
        mine = own
        if hop:
            mine = moved(own, lambda d: (d + hop * PLANE) % devices)
        pieces.append(mine)
        pieces.append(moved(mine, lambda d: d ^ 1))
    return pieces


def layer(
    tokens, attn_norm_gain, w_query, w_key, w_value, w_forget, forget_bias, w_attn_out,
    cache_keys, cache_values, cache_logcum, cache_lengths, expert_norm_gain, expert_ids,
    expert_weights, w_expert_gate, w_expert_up, w_expert_down, w_dense_gate, w_dense_up,
    w_dense_down, dense_norm_gain, branch_gate,
):
    devices = lax.axis_size("ep")
    own = jnp.concatenate([w_dense_gate.T, w_dense_up.T, w_dense_down], axis=0)
    pieces = gather_pieces(own, devices)
    mixed, branch, place, outgoing = mixer(
        tokens, attn_norm_gain, w_query, w_key, w_value, w_forget, forget_bias, w_attn_out,
        cache_keys, cache_values, cache_logcum, cache_lengths, expert_norm_gain, branch_gate,
        expert_ids, expert_weights, devices)
    arrived = lax.all_to_all(outgoing, "ep", split_axis=0, concat_axis=0, tiled=True)
    me = lax.axis_index("ep").astype(jnp.int32).reshape(1)
    answer = worker(me, arrived, w_expert_gate, w_expert_up, w_expert_down, pieces, dense_norm_gain)
    returned = lax.all_to_all(answer, "ep", split_axis=0, concat_axis=0, tiled=True)
    return merger(returned, place, mixed, branch)


def solution(mesh):
    in_specs = (
        P("ep", None),
        P(),
        P(),
        P(),
        P(),
        P(),
        P(),
        P(),
        P("ep", None, None),
        P("ep", None, None),
        P("ep", None, None),
        P("ep"),
        P(),
        P("ep", None),
        P("ep", None),
        P("ep", None, None),
        P("ep", None, None),
        P("ep", None, None),
        P(None, "ep"),
        P(None, "ep"),
        P("ep", None),
        P(),
        P(),
    )
    out_specs = P("ep", None)
    return jax.shard_map(
        layer, mesh=mesh, in_specs=in_specs, out_specs=out_specs, check_vma=False)
```

profile of v0, /device:TPU:1, one launch (start us, length us, event | category | flops | bytes accessed | tf_op | source)
XLA Modules:
  0.0 126.1 jit_solution(6732988622173010022)
XLA Ops:
  0.0 11.4 %mixer.1 = (bf16[18,2048]{1,0:T(8,128)(2,1)S(1)}, f32[18,128]{1,0:T(8,128)S(1)}, f32[256,18]{1,0:T(8,128)S(1)}, bf16[128,2,5120]{2,1,0:T(2,128)(2,1)}) custom-call(bf16[18,2048]{1,0:T(8,128)(2,1)} %tokens_hbm.1, f32[1,2048]{1,0:T(1,128)} %bitcast.16, bf16[2048,512]{1,0:T(8,128)(2,1)} %wq_hbm.1, bf16[2048,128]{1,0:T(8,128)(2,1)} %wk_hbm.1, ...), custom_call_target="tpu_custom_call" | custom-call | flops 10000000000 | bytes 15728640 | tf_op jit(solution)/shard_map/mixer/pallas_call | solution.py:205
  11.4 0.0 copy-start.2
  11.4 0.0 copy-start.3
  11.4 0.0 copy-start
  11.5 11.5 %all-to-all-start = ((bf16[128,2,5120]{2,1,0:T(2,128)(2,1)}), bf16[128,2,5120]{2,1,0:T(2,128)(2,1)S(1)}, u32[]{:S(2)}, u32[]{:S(2)}) async-start(bf16[128,2,5120]{2,1,0:T(2,128)(2,1)} %get-tuple-element.9), calls=%async_computation | async-start | bytes 5242880 | tf_op jit(solution)/shard_map/all_to_all | solution.py:402
  23.0 0.9 pad_maximum_fusion.h0
  23.9 3.3 %collective-permute-start.5 = (bf16[96,2048]{1,0:T(8,128)(2,1)S(1)}, bf16[96,2048]{1,0:T(8,128)(2,1)}, u32[]{:S(2)}, u32[]{:S(2)}) collective-permute-start(bf16[96,2048]{1,0:T(8,128)(2,1)S(1)} %pad_maximum_fusion.h0), channel_id=1, source_target_pairs={{0,96},{1,97},{2,98},{3,99},{4,100},{5,101},{6,102},{7,103},{8,104... | collective-permute-start | bytes 1179656 | tf_op jit(solution)/shard_map/ppermute | solution.py:377
  27.2 0.1 collective-permute-start.3
  27.4 0.8 collective-permute-start.1
  28.1 1.2 collective-permute-start
  29.3 31.8 %collective-permute-done.5.h6 = bf16[96,2048]{1,0:T(8,128)(2,1)} collective-permute-done((bf16[96,2048]{1,0:T(8,128)(2,1)S(1)}, bf16[96,2048]{1,0:T(8,128)(2,1)}, u32[]{:S(2)}, u32[]{:S(2)}) %collective-permute-start.5) | collective-permute-done | bytes 393248 | tf_op jit(solution)/shard_map/ppermute | solution.py:377
  61.1 1.6 %collective-permute-start.6 = (bf16[96,2048]{1,0:T(8,128)(2,1)}, bf16[96,2048]{1,0:T(8,128)(2,1)}, u32[]{:S(2)}, u32[]{:S(2)}) collective-permute-start(bf16[96,2048]{1,0:T(8,128)(2,1)} %collective-permute-done.5.h6), channel_id=1, source_target_pairs={{0,1},{1,0},{2,3},{3,2},{4,5},{5,4},{6,7},{7,6},{8,9},{9,8},{10,11... | collective-permute-start | bytes 1179656 | tf_op jit(solution)/shard_map/ppermute | solution.py:377
  62.7 0.8 collective-permute-done.3.h4
  63.5 0.4 collective-permute-start.4
  63.9 8.0 %collective-permute-done.1.h2 = bf16[96,2048]{1,0:T(8,128)(2,1)} collective-permute-done((bf16[96,2048]{1,0:T(8,128)(2,1)S(1)}, bf16[96,2048]{1,0:T(8,128)(2,1)}, u32[]{:S(2)}, u32[]{:S(2)}) %collective-permute-start.1) | collective-permute-done | bytes 393248 | tf_op jit(solution)/shard_map/ppermute | solution.py:377
  71.9 0.4 collective-permute-start.2
  72.3 0.0 collective-permute-done.h1
  72.3 0.0 collective-permute-done.6.h7
  72.3 0.0 collective-permute-done.4.h5
  72.3 1.7 %collective-permute-done.2.h3 = bf16[96,2048]{1,0:T(8,128)(2,1)} collective-permute-done((bf16[96,2048]{1,0:T(8,128)(2,1)}, bf16[96,2048]{1,0:T(8,128)(2,1)}, u32[]{:S(2)}, u32[]{:S(2)}) %collective-permute-start.2) | collective-permute-done | bytes 393248 | tf_op jit(solution)/shard_map/ppermute | solution.py:377
  74.0 0.0 all-to-all-done.arrived_ref
  74.0 6.1 %worker.1 = bf16[128,2,5248]{2,1,0:T(2,128)(2,1)S(1)} custom-call(s32[1]{0:T(128)} %bitcast.device_ref, bf16[128,2,5120]{2,1,0:T(2,128)(2,1)S(1)} %all-to-all-done.arrived_ref, bf16[1,2048,512]{2,1,0:T(8,128)(2,1)} %gate_hbm.1, bf16[1,2048,512]{2,1,0:T(8,128)(2,1)} %up_hbm.1, bf16[1,512,2048]{2,1,0:T(8,128)(2,1)} %down_hbm.1, bf16[96,2048]{1,0:T(8,128)(2,1)} %copy-done.1, ...), custom_call_target="tpu_custom_call" | custom-call | flops 5000000000 | bytes 15728640 | tf_op jit(solution)/shard_map/worker/pallas_call | solution.py:315
  80.1 44.2 %all_to_all.10.returned_ref = bf16[128,2,5248]{2,1,0:T(2,128)(2,1)S(1)} all-to-all(bf16[128,2,5248]{2,1,0:T(2,128)(2,1)S(1)} %worker.1), channel_id=1, replica_groups=mesh['ep'=128] {'ep'}, dimensions={0} | all-to-all | bytes 5373952 | tf_op jit(solution)/shard_map/all_to_all | solution.py:405
  124.3 1.9 %merger.1 = bf16[18,2048]{1,0:T(8,128)(2,1)} custom-call(bf16[128,2,5248]{2,1,0:T(2,128)(2,1)S(1)} %all_to_all.10.returned_ref, f32[256,18]{1,0:T(8,128)S(1)} %get-tuple-element.10.place_ref, bf16[18,2048]{1,0:T(8,128)(2,1)S(1)} %get-tuple-element.11.mixed_ref, f32[18,128]{1,0:T(8,128)S(1)} %get-tuple-element.12.branch_ref), custom_call_target="tpu_custom_call" | custom-call | tf_op jit(solution)/shard_map/merger/pallas_call | solution.py:365
  (5 shorter events, 0.0 us)
Async XLA Ops:
  11.4 11.5 %copy-start.2 = (bf16[32,2048]{1,0:T(8,128)(2,1)S(1)}, bf16[32,2048]{1,0:T(8,128)(2,1)}, u32[]{:S(2)}) copy-start(bf16[32,2048]{1,0:T(8,128)(2,1)} %param.43) | copy-start | bytes 393220
  11.4 11.5 %copy-start.3 = (bf16[2048,32]{0,1:T(8,128)(2,1)S(1)}, bf16[2048,32]{0,1:T(8,128)(2,1)}, u32[]{:S(2)}) copy-start(bf16[2048,32]{0,1:T(8,128)(2,1)} %param.42) | copy-start | bytes 393220
  11.4 62.6 %copy-start = (f32[4096]{0:T(1024)S(1)}, f32[4096]{0:T(1024)}, u32[]{:S(2)}) copy-start(f32[4096]{0:T(1024)} %param.44) | copy-start | bytes 49156
  11.5 62.5 %all-to-all-start = ((bf16[128,2,5120]{2,1,0:T(2,128)(2,1)}), bf16[128,2,5120]{2,1,0:T(2,128)(2,1)S(1)}, u32[]{:S(2)}, u32[]{:S(2)}) async-start(bf16[128,2,5120]{2,1,0:T(2,128)(2,1)} %get-tuple-element.9), calls=%async_computation | async-start | bytes 5242880 | tf_op jit(solution)/shard_map/all_to_all | solution.py:402
  23.9 50.1 %copy-start.1 = (bf16[96,2048]{1,0:T(8,128)(2,1)}, bf16[96,2048]{1,0:T(8,128)(2,1)S(1)}, u32[]{:S(2)}) copy-start(bf16[96,2048]{1,0:T(8,128)(2,1)S(1)} %pad_maximum_fusion.h0) | copy-start | bytes 1179652
  23.9 37.2 %collective-permute-start.5 = (bf16[96,2048]{1,0:T(8,128)(2,1)S(1)}, bf16[96,2048]{1,0:T(8,128)(2,1)}, u32[]{:S(2)}, u32[]{:S(2)}) collective-permute-start(bf16[96,2048]{1,0:T(8,128)(2,1)S(1)} %pad_maximum_fusion.h0), channel_id=1, source_target_pairs={{0,96},{1,97},{2,98},{3,99},{4,100},{5,101},{6,102},{7,103},{8,104... | collective-permute-start | bytes 1179656 | tf_op jit(solution)/shard_map/ppermute | solution.py:377
  27.2 36.2 %collective-permute-start.3 = (bf16[96,2048]{1,0:T(8,128)(2,1)S(1)}, bf16[96,2048]{1,0:T(8,128)(2,1)}, u32[]{:S(2)}, u32[]{:S(2)}) collective-permute-start(bf16[96,2048]{1,0:T(8,128)(2,1)S(1)} %pad_maximum_fusion.h0), channel_id=1, source_target_pairs={{0,64},{1,65},{2,66},{3,67},{4,68},{5,69},{6,70},{7,71},{8,72},{9,... | collective-permute-start | bytes 1179656 | tf_op jit(solution)/shard_map/ppermute | solution.py:377
  27.4 44.5 %collective-permute-start.1 = (bf16[96,2048]{1,0:T(8,128)(2,1)S(1)}, bf16[96,2048]{1,0:T(8,128)(2,1)}, u32[]{:S(2)}, u32[]{:S(2)}) collective-permute-start(bf16[96,2048]{1,0:T(8,128)(2,1)S(1)} %pad_maximum_fusion.h0), channel_id=1, source_target_pairs={{0,32},{1,33},{2,34},{3,35},{4,36},{5,37},{6,38},{7,39},{8,40},{9,... | collective-permute-start | bytes 1179656 | tf_op jit(solution)/shard_map/ppermute | solution.py:377
  28.1 44.2 %collective-permute-start = (bf16[96,2048]{1,0:T(8,128)(2,1)S(1)}, bf16[96,2048]{1,0:T(8,128)(2,1)}, u32[]{:S(2)}, u32[]{:S(2)}) collective-permute-start(bf16[96,2048]{1,0:T(8,128)(2,1)S(1)} %pad_maximum_fusion.h0), channel_id=1, source_target_pairs={{0,1},{1,0},{2,3},{3,2},{4,5},{5,4},{6,7},{7,6},{8,9},{9,8},{10,11... | collective-permute-start | bytes 1179656 | tf_op jit(solution)/shard_map/ppermute | solution.py:377
  61.1 11.2 %collective-permute-start.6 = (bf16[96,2048]{1,0:T(8,128)(2,1)}, bf16[96,2048]{1,0:T(8,128)(2,1)}, u32[]{:S(2)}, u32[]{:S(2)}) collective-permute-start(bf16[96,2048]{1,0:T(8,128)(2,1)} %collective-permute-done.5.h6), channel_id=1, source_target_pairs={{0,1},{1,0},{2,3},{3,2},{4,5},{5,4},{6,7},{7,6},{8,9},{9,8},{10,11... | collective-permute-start | bytes 1179656 | tf_op jit(solution)/shard_map/ppermute | solution.py:377
  63.5 8.9 %collective-permute-start.4 = (bf16[96,2048]{1,0:T(8,128)(2,1)}, bf16[96,2048]{1,0:T(8,128)(2,1)}, u32[]{:S(2)}, u32[]{:S(2)}) collective-permute-start(bf16[96,2048]{1,0:T(8,128)(2,1)} %collective-permute-done.3.h4), channel_id=1, source_target_pairs={{0,1},{1,0},{2,3},{3,2},{4,5},{5,4},{6,7},{7,6},{8,9},{9,8},{10,11... | collective-permute-start | bytes 1179656 | tf_op jit(solution)/shard_map/ppermute | solution.py:377
  71.9 2.1 %collective-permute-start.2 = (bf16[96,2048]{1,0:T(8,128)(2,1)}, bf16[96,2048]{1,0:T(8,128)(2,1)}, u32[]{:S(2)}, u32[]{:S(2)}) collective-permute-start(bf16[96,2048]{1,0:T(8,128)(2,1)} %collective-permute-done.1.h2), channel_id=1, source_target_pairs={{0,1},{1,0},{2,3},{3,2},{4,5},{5,4},{6,7},{7,6},{8,9},{9,8},{10,11... | collective-permute-start | bytes 1179656 | tf_op jit(solution)/shard_map/ppermute | solution.py:377
where the time goes:
time: 126 us
  blocking collectives  44.2 us (35%)
  waiting for transfers between devices  42.2 us (33%)
  Pallas kernels  19.3 us (15%)
  starting transfers between devices  19.3 us (15%)
    all_to_all x1, blocking collectives, layer(): lax.all_to_all(answer, 'ep', split_axis=0, concat_axis=0, tiled=True)  44.2 us
    ppermute x7, waiting for transfers between devices, moved(): return lax.ppermute(array, 'ep', [(d, target(d)) for d in range(devices)])  42.2 us
    all_to_all x1, starting transfers between devices, layer(): lax.all_to_all(outgoing, 'ep', split_axis=0, concat_axis=0, tiled=True)  11.5 us
    pallas_call x1, Pallas kernels, mixer(): pl.pallas_call(mixer_body, out_shape=(jax.ShapeDtypeStruct((seqs, width),...  11.4 us
    ppermute x7, starting transfers between devices, moved(): return lax.ppermute(array, 'ep', [(d, target(d)) for d in range(devices)])  7.85 us
    pallas_call x1, Pallas kernels, worker(): pl.pallas_call(worker_body, out_shape=jax.ShapeDtypeStruct((devices, cap,...  6.07 us
  transfers between devices with their start and end apart: 8, of which 4 were waited for; matrix products, arithmetic and copies ran while one was open for 1% of the time, Pallas kernels for 0%

commit v1 on v0

--- a/solution.py
+++ b/solution.py
@@ -17,6 +17,7 @@
 PLANE = 32
 CORES = 2
 PARTS = 8
+SIDE = 4
 DENSE_FF = 4096
 F32 = jnp.float32
 BF16 = jnp.bfloat16
@@ -30,27 +31,15 @@
     return jnp.dot(a, b, preferred_element_type=F32)
 
 
-def slot_masks(slots, seqs):
+def fill_outgoing(routed_in, ids_ref, eweights_ref, place_ref, outgoing_ref):
+    seqs, width = routed_in.shape
+    devices = outgoing_ref.shape[0]
+    slots = devices * CAP
     slot = lax.broadcasted_iota(jnp.int32, (slots, seqs), 0)
-    token = lax.broadcasted_iota(jnp.int32, (slots, seqs), 1)
-    device = slot // CAP
-    part = (device // PLANE) * CORES + device % CORES
-    dense = token == part + PARTS * (slot % CAP)
-    extra = token == part + PARTS * CAP
-    return slot, device, dense, extra
-
-
-def fill_outgoing(
-    routed_in, ids_ref, eweights_ref, place_ref, outgoing_ref, outgoing_hbm, out_sems
-):
-    seqs, width = routed_in.shape
-    half = width // CAP
-    slots = outgoing_ref.shape[0] * CAP
-    slot, device, dense, extra = slot_masks(slots, seqs)
     member = jnp.zeros((slots, seqs), F32)
     share = jnp.zeros((slots, seqs), F32)
     for k in range(TOPK):
-        hit = ids_ref[k:k + 1, :] == device
+        hit = ids_ref[k:k + 1, :] == slot // CAP
         member = member + jnp.where(hit, 1.0, 0.0)
         share = share + jnp.where(hit, eweights_ref[k:k + 1, :], 0.0)
     earlier = lax.broadcasted_iota(jnp.int32, (seqs, seqs), 0)
@@ -60,33 +49,15 @@
     here = prior == (slot % CAP).astype(F32)
     place_ref[...] = jnp.where(here, share, 0.0)
     routes = jnp.where(here, member, 0.0).astype(BF16)
-    extra = jnp.where(extra, 1.0, 0.0).astype(BF16)
-    even = lax.broadcasted_iota(jnp.int32, (slots, half), 0) % CAP == 0
-    third = jnp.where(even, dot(extra, routed_in[:, :half]), dot(extra, routed_in[:, half:]))
-    devices = slots // CAP
-    copies = []
-
-    def send(start, stop, value):
-        window = (slice(None), slice(None), pl.ds(start, stop - start))
-        outgoing_ref[window] = value.astype(BF16).reshape(devices, CAP, stop - start)
-        copies.append(pltpu.make_async_copy(
-            outgoing_ref.at[window], outgoing_hbm.at[window], out_sems.at[len(copies)]))
-        copies[-1].start()
-
-    send(2 * width, 2 * width + half, third)
-    send(width, 2 * width, dot(jnp.where(dense, 1.0, 0.0).astype(BF16), routed_in))
-    send(0, width, dot(routes, routed_in))
-    for copy in copies:
-        copy.wait()
+    outgoing_ref[...] = dot(routes, routed_in).astype(BF16).reshape(devices, CAP, width)
 
 
 def mixer_body(
     tokens_hbm, again_hbm, wq_hbm, wk_hbm, wv_hbm, wf_hbm, fbias_hbm, wo_hbm,
     keys_hbm, values_hbm, logcum_hbm, lengths_hbm, egain_hbm, bgate_hbm, ids_hbm, eweights_hbm,
-    mixed_ref, branch_ref, place_ref, outgoing_hbm,
+    mixed_ref, routed_ref, branch_ref, place_ref, outgoing_ref,
     tokens_ref, again_ref, wq, wk, wv, wf_ref, fbias_ref, wo,
     kbuf, vbuf, cbuf, lengths_ref, egain_ref, bgate_ref, ids_ref, eweights_ref, sems,
-    outgoing_ref, out_sems,
 ):
     sources = dict(
         tokens=(tokens_hbm, tokens_ref), again=(again_hbm, again_ref), wf=(wf_hbm, wf_ref),
@@ -188,8 +159,8 @@
     routed_in = (y * scale * egain_ref[...]).astype(BF16)
     branch = jax.nn.sigmoid(jnp.sum(routed_in.astype(F32) * bgate_ref[...], axis=1, keepdims=True))
     branch_ref[...] = jnp.broadcast_to(branch, branch_ref.shape)
-    fill_outgoing(
-        routed_in, ids_ref, eweights_ref, place_ref, outgoing_ref, outgoing_hbm, out_sems)
+    routed_ref[...] = routed_in
+    fill_outgoing(routed_in, ids_ref, eweights_ref, place_ref, outgoing_ref)
 
 
 def mixer(tokens, attn_norm_gain, w_query, w_key, w_value, w_forget, forget_bias, w_attn_out,
@@ -206,54 +177,72 @@
         mixer_body,
         out_shape=(
             jax.ShapeDtypeStruct((seqs, width), BF16),
+            jax.ShapeDtypeStruct((seqs, width), BF16),
             jax.ShapeDtypeStruct((seqs, 128), F32),
             jax.ShapeDtypeStruct((devices * CAP, seqs), F32),
-            pltpu.HBM((devices, CAP, 2 * width + width // CAP), BF16),
+            jax.ShapeDtypeStruct((devices, CAP, width), BF16),
         ),
         in_specs=[HBM] * len(operands),
-        out_specs=(VMEM, VMEM, VMEM, HBM),
+        out_specs=(VMEM,) * 5,
         scratch_shapes=[pltpu.VMEM(a.shape, a.dtype) for a in operands]
-        + [
-            pltpu.SemaphoreType.DMA((len(operands),)),
-            pltpu.VMEM((devices, CAP, 2 * width + width // CAP), BF16),
-            pltpu.SemaphoreType.DMA((3,)),
-        ],
+        + [pltpu.SemaphoreType.DMA((len(operands),))],
         compiler_params=pltpu.CompilerParams(vmem_limit_bytes=28 * 1024 * 1024),
         cost_estimate=pl.CostEstimate(flops=10**10, bytes_accessed=15 * 2**20, transcendentals=0),
         name="mixer",
     )(*operands)
 
 
-def pair(a):
-    return a.reshape(a.shape[0] // CAP, CAP, a.shape[1])
-
-
-def worker_body(
-    device_ref, arrived_ref, gate_hbm, up_hbm, down_hbm,
-    h0, h1, h2, h3, h4, h5, h6, h7, gain_ref,
-    answer_ref, wg, wu, wd, held, sems,
-):
-    devices, cap, _ = arrived_ref.shape
+def worker_body(arrived_ref, gate_hbm, up_hbm, down_hbm, answer_ref, wg, wu, wd, sems):
+    devices, cap, width = arrived_ref.shape
     rows = devices * cap
-    width = wd.shape[1]
-    half = width // CAP
-    weight_copies = [
+    copies = [
         pltpu.make_async_copy(source.at[0], target, sems.at[i])
         for i, (source, target) in enumerate(((gate_hbm, wg), (up_hbm, wu), (down_hbm, wd)))]
-    piece_copies = [
-        pltpu.make_async_copy(source, held.at[i], sems.at[3 + i])
-        for i, source in enumerate((h0, h1, h2, h3, h4, h5, h6, h7))]
-    for copy in weight_copies + piece_copies:
+    for copy in copies:
         copy.start()
-    x = arrived_ref[:, :, :width].reshape(rows, width)
-    weight_copies[0].wait()
+    x = arrived_ref[...].reshape(rows, width)
+    copies[0].wait()
     gate = jnp.minimum(dot(x, wg[...]), LIMIT)
-    weight_copies[1].wait()
+    copies[1].wait()
     up = jnp.clip(dot(x, wu[...]), -LIMIT, LIMIT)
     act = ((up + 1.0) * gate * jax.nn.sigmoid(gate * ALPHA)).astype(BF16)
-    weight_copies[2].wait()
-    answer_ref[:, :, :width] = pair(dot(act, wd[...]).astype(BF16))
-
+    copies[2].wait()
+    answer_ref[...] = dot(act, wd[...]).astype(BF16).reshape(devices, cap, width)
+
+
+def worker(arrived, gate_w, up_w, down_w):
+    stored = tuple(
+        pltpu.with_memory_space_constraint(a, pltpu.HBM) for a in (gate_w, up_w, down_w))
+    return pl.pallas_call(
+        worker_body,
+        out_shape=jax.ShapeDtypeStruct(arrived.shape, BF16),
+        in_specs=[VMEM] + [HBM] * 3,
+        out_specs=VMEM,
+        scratch_shapes=[pltpu.VMEM(a.shape[1:], BF16) for a in stored]
+        + [pltpu.SemaphoreType.DMA((3,))],
+        compiler_params=pltpu.CompilerParams(vmem_limit_bytes=20 * 1024 * 1024),
+        cost_estimate=pl.CostEstimate(flops=3 * 10**9, bytes_accessed=8 * 2**20, transcendentals=0),
+        name="worker",
+    )(arrived, *stored)
+
+
+def two_parts(square, rows):
+    lane = lax.broadcasted_iota(jnp.int32, (rows, 128), 1)
+    top = square.astype(BF16).astype(F32)
+    return jnp.where(lane == 0, top, jnp.where(lane == 1, square - top, 0.0))
+
+
+def dense_body(
+    device_ref, rows_ref, h0, h1, h2, h3, h4, h5, h6, h7, gain_ref,
+    o0, o1, o2, o3, held, sems,
+):
+    rows, width = rows_ref.shape
+    devices = PLANE * SIDE
+    copies = [
+        pltpu.make_async_copy(source, held.at[i], sems.at[i])
+        for i, source in enumerate((h0, h1, h2, h3, h4, h5, h6, h7))]
+    for copy in copies:
+        copy.start()
     units = held.shape[1] // 3
     me = device_ref[0]
     gains = []
@@ -263,7 +252,7 @@
         vec = jnp.zeros((1, 128), F32)
         for q in range(per_row):
             p = block * per_row + q
-            owner = lax.rem(me + (PARTS // CORES - p // CORES) * PLANE, devices)
+            owner = lax.rem(me + (SIDE - p // CORES) * PLANE, devices)
             if p % CORES:
                 owner = owner + 1 - 2 * lax.rem(me, CORES)
             line = gain_ref[pl.ds(owner // per_row, 1), :]
@@ -271,105 +260,111 @@
             vec = jnp.where(lane // units == q, pltpu.roll(line, shift, 1), vec)
         gains.append(vec)
     gain = jnp.concatenate(gains, axis=1)
-    for copy in piece_copies:
+    for copy in copies:
         copy.wait()
     dg = jnp.concatenate([held[p, :units] for p in range(PARTS)], axis=0)
     du = jnp.concatenate([held[p, units:2 * units] for p in range(PARTS)], axis=0)
     dd = jnp.concatenate([held[p, 2 * units:] for p in range(PARTS)], axis=0)
-
-    def nt(a, b):
-        return lax.dot_general(a, b, NT, preferred_element_type=F32)
-
-    def hidden_of(gate, up):
-        kept = (jax.nn.silu(gate) * up).astype(BF16).astype(F32)
-        square = jnp.sum(kept * kept, axis=1, keepdims=True)
-        return (kept * gain).astype(BF16), square
-
-    first = arrived_ref[:, :, width:2 * width].reshape(rows, width)
-    extra = arrived_ref[:, :, 2 * width:].reshape(rows, half)
-    hid, square = hidden_of(nt(first, dg), nt(first, du))
-    answer_ref[:, :, width:2 * width] = pair(dot(hid, dd).astype(BF16))
-    even = lax.broadcasted_iota(jnp.int32, (rows, PARTS * units), 0) % CAP == 0
-
-    def joined(weight):
-        both = jnp.where(even, nt(extra, weight[:, :half]), nt(extra, weight[:, half:]))
-        return both + pltpu.roll(both, rows - 1, 0)
-
-    hid3, square3 = hidden_of(joined(dg), joined(du))
-    low = dot(hid3, dd[:, :half])
-    high = pltpu.roll(dot(hid3, dd[:, half:]), 1, 0)
-    even = lax.broadcasted_iota(jnp.int32, (rows, half), 0) % CAP == 0
-    answer_ref[:, :, 2 * width:2 * width + half] = pair(jnp.where(even, low, high).astype(BF16))
-    lane = lax.broadcasted_iota(jnp.int32, (rows, 128), 1)
-    head = jnp.where(lane < 2, square, square3)
-    top = head.astype(BF16).astype(F32)
-    tail = jnp.where(lane % 2 == 0, top, head - top)
-    answer_ref[:, :, 2 * width + half:] = pair(jnp.where(lane < 4, tail, 0.0).astype(BF16))
-
-
-def worker(device, arrived, gate_w, up_w, down_w, pieces, gain):
-    devices, cap, packed = arrived.shape
-    stored = tuple(
-        pltpu.with_memory_space_constraint(a, pltpu.HBM) for a in (gate_w, up_w, down_w))
+    x = rows_ref[...]
+    gate = lax.dot_general(x, dg, NT, preferred_element_type=F32)
+    up = lax.dot_general(x, du, NT, preferred_element_type=F32)
+    kept = (jax.nn.silu(gate) * up).astype(BF16).astype(F32)
+    square = jnp.sum(kept * kept, axis=1, keepdims=True)
+    total = dot((kept * gain).astype(BF16), dd)
+    parts = two_parts(square, rows)
+    step = rows // SIDE
+    for k, out in enumerate((o0, o1, o2, o3)):
+        out[:, :width] = total[k * step:(k + 1) * step].astype(BF16)
+        out[:, width:] = parts[k * step:(k + 1) * step].astype(BF16)
+
+
+def dense_units(device, rows, pieces, gain):
     pieces = tuple(pltpu.with_memory_space_constraint(a, pltpu.HBM) for a in pieces)
+    count, width = rows.shape
     return pl.pallas_call(
-        worker_body,
-        out_shape=jax.ShapeDtypeStruct((devices, cap, packed + 128), BF16),
-        in_specs=[pl.BlockSpec(memory_space=pltpu.SMEM), VMEM] + [HBM] * 11 + [VMEM],
-        out_specs=VMEM,
-        scratch_shapes=[pltpu.VMEM(a.shape[1:], BF16) for a in stored]
-        + [
+        dense_body,
+        out_shape=tuple(
+            jax.ShapeDtypeStruct((count // SIDE, width + 128), BF16) for _ in range(SIDE)),
+        in_specs=[pl.BlockSpec(memory_space=pltpu.SMEM), VMEM] + [HBM] * len(pieces) + [VMEM],
+        out_specs=(VMEM,) * SIDE,
+        scratch_shapes=[
             pltpu.VMEM((len(pieces),) + pieces[0].shape, BF16),
-            pltpu.SemaphoreType.DMA((3 + len(pieces),)),
+            pltpu.SemaphoreType.DMA((len(pieces),)),
         ],
-        compiler_params=pltpu.CompilerParams(vmem_limit_bytes=28 * 1024 * 1024),
-        cost_estimate=pl.CostEstimate(flops=5 * 10**9, bytes_accessed=15 * 2**20, transcendentals=0),
-        name="worker",
-    )(device, arrived, *stored, *pieces, gain.reshape(-1, 128))
-
-
-def merger_body(returned_ref, place_ref, mixed_ref, branch_ref, result_ref):
-    devices, cap, _ = returned_ref.shape
-    seqs, width = mixed_ref.shape
+        compiler_params=pltpu.CompilerParams(vmem_limit_bytes=20 * 1024 * 1024),
+        cost_estimate=pl.CostEstimate(flops=2 * 10**9, bytes_accessed=6 * 2**20, transcendentals=0),
+        name="dense",
+    )(device, rows, *pieces, gain.reshape(-1, 128))
+
+
+def fold_body(a, b, c, d, o0, o1, o2, o3):
+    rows = a.shape[0]
+    width = a.shape[1] - 128
+    total = sum(r[:, :width].astype(F32) for r in (a, b, c, d))
+    squares = sum(r[:, width:].astype(F32) for r in (a, b, c, d))
+    parts = two_parts(jnp.sum(squares, axis=1, keepdims=True), rows)
+    step = rows // SIDE
+    for k, out in enumerate((o0, o1, o2, o3)):
+        out[:, :width] = total[k * step:(k + 1) * step].astype(BF16)
+        out[:, width:] = parts[k * step:(k + 1) * step].astype(BF16)
+
+
+def fold(blocks):
+    rows, packed = blocks[0].shape
+    return pl.pallas_call(
+        fold_body,
+        out_shape=tuple(jax.ShapeDtypeStruct((rows // SIDE, packed), BF16) for _ in range(SIDE)),
+        in_specs=[VMEM] * SIDE,
+        out_specs=(VMEM,) * SIDE,
+        compiler_params=pltpu.CompilerParams(vmem_limit_bytes=12 * 1024 * 1024),
+        name="fold",
+    )(*blocks)
+
+
+def merger_body(returned_ref, place_ref, mixed_ref, branch_ref, a, b, c, d, result_ref):
+    devices, cap, width = returned_ref.shape
     rows = devices * cap
-    half = width // CAP
+    total = sum(r[:, :width].astype(F32) for r in (a, b, c, d))
+    squares = sum(r[:, width:].astype(F32) for r in (a, b, c, d))
+    unit_scale = lax.rsqrt(jnp.sum(squares, axis=1, keepdims=True) / DENSE_FF + EPS)
+    base = mixed_ref[...].astype(F32) + branch_ref[:, :1] * (total * unit_scale)
 
     def tn(a, b):
         return lax.dot_general(a, b, TN, preferred_element_type=F32)
 
-    slot, _, dense, extra = slot_masks(rows, seqs)
     share = place_ref[...]
     s1 = share.astype(BF16)
     rest = share - s1.astype(F32)
     s2 = rest.astype(BF16)
     s3 = (rest - s2.astype(F32)).astype(BF16)
-    answers = returned_ref[:, :, :width].reshape(rows, width)
+    answers = returned_ref[...].reshape(rows, width)
     routed = tn(s1, answers) + tn(s2, answers) + tn(s3, answers)
-    dense = jnp.where(dense, 1.0, 0.0).astype(BF16)
-    low = jnp.where(extra & (slot % CAP == 0), 1.0, 0.0).astype(BF16)
-    high = jnp.where(extra & (slot % CAP == 1), 1.0, 0.0).astype(BF16)
-    total = tn(dense, returned_ref[:, :, width:2 * width].reshape(rows, width))
-    third = returned_ref[:, :, 2 * width:2 * width + half].reshape(rows, half)
-    total = total + jnp.concatenate([tn(low, third), tn(high, third)], axis=1)
-    sums = returned_ref[:, :, 2 * width + half:].reshape(rows, 128)
-    lane = lax.broadcasted_iota(jnp.int32, (seqs, 128), 1)
-    square = jnp.where(lane < 2, tn(dense, sums), 0.0)
-    square = square + jnp.where((lane >= 2) & (lane < 4), tn(low, sums), 0.0)
-    square = jnp.sum(square, axis=1, keepdims=True)
-    unit_scale = lax.rsqrt(square / DENSE_FF + EPS)
-    out = mixed_ref[...].astype(F32) + routed + branch_ref[:, :1] * (total * unit_scale)
-    result_ref[...] = out.astype(BF16)
-
-
-def merger(returned, place, mixed, branch):
+    result_ref[...] = (base + routed).astype(BF16)
+
+
+def merger(returned, place, mixed, branch, blocks):
     return pl.pallas_call(
         merger_body,
         out_shape=jax.ShapeDtypeStruct(mixed.shape, BF16),
-        in_specs=[VMEM] * 4,
+        in_specs=[VMEM] * (4 + SIDE),
         out_specs=VMEM,
         compiler_params=pltpu.CompilerParams(vmem_limit_bytes=16 * 1024 * 1024),
         name="merger",
-    )(returned, place, mixed, branch)
+    )(returned, place, mixed, branch, *blocks)
+
+
+def shifted(array, devices, stride, by):
+    ring = stride * SIDE
+    pairs = [
+        (d, d // ring * ring + (d % ring + by * stride) % ring) for d in range(devices)]
+    return lax.ppermute(array, "ep", pairs)
+
+
+def exchange(blocks, devices, stride, sign):
+    out = [blocks[0]]
+    for k in range(1, SIDE):
+        out.append(shifted(blocks[k], devices, stride, sign * k))
+    return out
 
 
 def gather_pieces(own, devices):
@@ -393,17 +388,24 @@
     w_dense_down, dense_norm_gain, branch_gate,
 ):
     devices = lax.axis_size("ep")
+    across, along = CORES, CORES * SIDE
+    me = lax.axis_index("ep").astype(jnp.int32).reshape(1)
     own = jnp.concatenate([w_dense_gate.T, w_dense_up.T, w_dense_down], axis=0)
     pieces = gather_pieces(own, devices)
-    mixed, branch, place, outgoing = mixer(
+    mixed, routed_in, branch, place, outgoing = mixer(
         tokens, attn_norm_gain, w_query, w_key, w_value, w_forget, forget_bias, w_attn_out,
         cache_keys, cache_values, cache_logcum, cache_lengths, expert_norm_gain, branch_gate,
         expert_ids, expert_weights, devices)
     arrived = lax.all_to_all(outgoing, "ep", split_axis=0, concat_axis=0, tiled=True)
-    me = lax.axis_index("ep").astype(jnp.int32).reshape(1)
-    answer = worker(me, arrived, w_expert_gate, w_expert_up, w_expert_down, pieces, dense_norm_gain)
+    row = jnp.concatenate(exchange([routed_in] * SIDE, devices, across, 1), axis=0)
+    rows = jnp.concatenate(exchange([row] * SIDE, devices, along, 1), axis=0)
+    partial = dense_units(me, rows, pieces, dense_norm_gain)
+    partial = exchange(partial, devices, along, -1)
+    partial = fold(partial)
+    partial = exchange(partial, devices, across, -1)
+    answer = worker(arrived, w_expert_gate, w_expert_up, w_expert_down)
     returned = lax.all_to_all(answer, "ep", split_axis=0, concat_axis=0, tiled=True)
-    return merger(returned, place, mixed, branch)
+    return merger(returned, place, mixed, branch, partial)
 
 
 def solution(mesh):

time: 126 us -> 117 us (0.929)
  blocking collectives: 44.2 us -> 0 us
  starting transfers between devices: 19.3 us -> 44.7 us
  local copies, waits for them, and re-layouts: 0.02 us -> 6.07 us
  waiting for transfers between devices: 42.2 us -> 45.1 us
    ppermute x0 -> x12, waiting for transfers between devices: none -> 45.1 us  [shifted(): return lax.ppermute(array, 'ep', pairs)]
    all_to_all x1 -> x0, blocking collectives: 44.2 us -> none  [layer(): lax.all_to_all(answer, 'ep', split_axis=0, concat_axis=0, tiled=True)]
    ppermute x7, waiting for transfers between devices: 42.2 us -> 0.02 us  [moved(): return lax.ppermute(array, 'ep', [(d, target(d)) for d in range(devices)])]
    ppermute x0 -> x12, starting transfers between devices: none -> 17.5 us  [shifted(): return lax.ppermute(array, 'ep', pairs)]
    all_to_all x0 -> x1, starting transfers between devices: none -> 6.41 us  [layer(): lax.all_to_all(answer, 'ep', split_axis=0, concat_axis=0, tiled=True)]
    concatenate x0 -> x1, local copies, waits for them, and re-layouts: none -> 6.03 us  [layer(): rows = jnp.concatenate(exchange([row] * SIDE, devices, along, 1), axis=0)]
    pallas_call x1 -> x3, Pallas kernels: 6.07 us -> 8.28 us  [the longest x1 4.81 us: worker(): pl.pallas_call(worker_body, out_shape=jax.ShapeDtypeStruct(arrived.shape,...]
    ppermute x7, starting transfers between devices: 7.85 us -> 9.23 us  [moved(): return lax.ppermute(array, 'ep', [(d, target(d)) for d in range(devices)])]
  transfers between devices with their start and end apart: 8 -> 21, of which waited for: 4 -> 8; matrix products, arithmetic and copies ran while one was open for 1% -> 5% of each run, Pallas kernels for 0% -> 7%
where the time goes in v1:
time: 117 us; the launch traced here: 116 us
  waiting for transfers between devices  45.1 us (39%)
  starting transfers between devices  44.7 us (38%)
  Pallas kernels  20.2 us (17%)
  local copies, waits for them, and re-layouts  6.07 us (5%)
    ppermute x12, waiting for transfers between devices, shifted(): return lax.ppermute(array, 'ep', pairs)  45.1 us
    ppermute x12, starting transfers between devices, shifted(): return lax.ppermute(array, 'ep', pairs)  17.5 us
    all_to_all x1, starting transfers between devices, layer(): lax.all_to_all(outgoing, 'ep', split_axis=0, concat_axis=0, tiled=True)  11.5 us
    pallas_call x1, Pallas kernels, mixer(): pl.pallas_call(mixer_body, out_shape=(jax.ShapeDtypeStruct((seqs, width),...  10.6 us
    ppermute x7, starting transfers between devices, moved(): return lax.ppermute(array, 'ep', [(d, target(d)) for d in range(devices)])  9.23 us
    all_to_all x1, starting transfers between devices, layer(): lax.all_to_all(answer, 'ep', split_axis=0, concat_axis=0, tiled=True)  6.41 us
    concatenate x1, local copies, waits for them, and re-layouts, layer(): rows = jnp.concatenate(exchange([row] * SIDE, devices, along, 1), axis=0)  6.03 us
    pallas_call x1, Pallas kernels, worker(): pl.pallas_call(worker_body, out_shape=jax.ShapeDtypeStruct(arrived.shape,...  4.81 us
  transfers between devices with their start and end apart: 21, of which 8 were waited for; matrix products, arithmetic and copies ran while one was open for 5% of the time, Pallas kernels for 7%

profile of v1, /device:TPU:1, one launch (start us, length us, event | category | flops | bytes accessed | tf_op | source)
XLA Modules:
  0.0 116.4 jit_solution(4888823293126929457)
XLA Ops:
  0.0 10.6 %mixer.1 = (bf16[18,2048]{1,0:T(8,128)(2,1)S(1)}, bf16[18,2048]{1,0:T(8,128)(2,1)S(1)}, f32[18,128]{1,0:T(8,128)S(1)}, f32[256,18]{1,0:T(8,128)S(1)}, bf16[128,2,2048]{2,1,0:T(2,128)(2,1)}) custom-call(bf16[18,2048]{1,0:T(8,128)(2,1)} %tokens_hbm.1, f32[1,2048]{1,0:T(1,128)} %bitcast.16, bf16[2048,512]{1,0:T(8,128)(2,1)} %wq_hbm.1, ...), custom_call_target="tpu_custom_call" | custom-call | flops 10000000000 | bytes 15728640 | tf_op jit(solution)/shard_map/mixer/pallas_call | solution.py:176
  10.6 11.5 %all-to-all-start = ((bf16[128,2,2048]{2,1,0:T(2,128)(2,1)}), bf16[128,2,2048]{2,1,0:T(2,128)(2,1)S(1)}, u32[]{:S(2)}, u32[]{:S(2)}) async-start(bf16[128,2,2048]{2,1,0:T(2,128)(2,1)} %get-tuple-element.18), calls=%async_computation | async-start | bytes 2097152 | tf_op jit(solution)/shard_map/all_to_all | solution.py:399
  22.1 1.4 %collective-permute-start = (bf16[18,2048]{1,0:T(8,128)(2,1)S(1)}, bf16[18,2048]{1,0:T(8,128)(2,1)S(1)}, u32[]{:S(2)}, u32[]{:S(2)}) collective-permute-start(bf16[18,2048]{1,0:T(8,128)(2,1)S(1)} %get-tuple-element.22), channel_id=1, source_target_pairs={{0,2},{1,3},{2,4},{3,5},{4,6},{5,7},{6,0},{7,1},{8,10},{9,11},{10,... | collective-permute-start | bytes 221192 | tf_op jit(solution)/shard_map/ppermute | solution.py:360
  23.6 2.4 %collective-permute-start.1 = (bf16[18,2048]{1,0:T(8,128)(2,1)S(1)}, bf16[18,2048]{1,0:T(8,128)(2,1)S(1)}, u32[]{:S(2)}, u32[]{:S(2)}) collective-permute-start(bf16[18,2048]{1,0:T(8,128)(2,1)S(1)} %get-tuple-element.22), channel_id=1, source_target_pairs={{0,4},{1,5},{2,6},{3,7},{4,0},{5,1},{6,2},{7,3},{8,12},{9,13},{10,... | collective-permute-start | bytes 221192 | tf_op jit(solution)/shard_map/ppermute | solution.py:360
  27.2 1.4 %collective-permute-start.7 = (bf16[96,2048]{1,0:T(8,128)(2,1)S(1)}, bf16[96,2048]{1,0:T(8,128)(2,1)}, u32[]{:S(2)}, u32[]{:S(2)}) collective-permute-start(bf16[96,2048]{1,0:T(8,128)(2,1)S(1)} %pad_maximum_fusion.h0), channel_id=1, source_target_pairs={{0,32},{1,33},{2,34},{3,35},{4,36},{5,37},{6,38},{7,39},{8,40},{9,... | collective-permute-start | bytes 1179656 | tf_op jit(solution)/shard_map/ppermute | solution.py:372
  28.6 2.9 %collective-permute-start.9 = (bf16[96,2048]{1,0:T(8,128)(2,1)S(1)}, bf16[96,2048]{1,0:T(8,128)(2,1)}, u32[]{:S(2)}, u32[]{:S(2)}) collective-permute-start(bf16[96,2048]{1,0:T(8,128)(2,1)S(1)} %pad_maximum_fusion.h0), channel_id=1, source_target_pairs={{0,64},{1,65},{2,66},{3,67},{4,68},{5,69},{6,70},{7,71},{8,72},{9,... | collective-permute-start | bytes 1179656 | tf_op jit(solution)/shard_map/ppermute | solution.py:372
  31.5 6.6 %collective-permute-done = bf16[18,2048]{1,0:T(8,128)(2,1)S(1)} collective-permute-done((bf16[18,2048]{1,0:T(8,128)(2,1)S(1)}, bf16[18,2048]{1,0:T(8,128)(2,1)S(1)}, u32[]{:S(2)}, u32[]{:S(2)}) %collective-permute-start) | collective-permute-done | bytes 73760 | tf_op jit(solution)/shard_map/ppermute | solution.py:360
  38.2 3.1 %collective-permute-start.11 = (bf16[96,2048]{1,0:T(8,128)(2,1)S(1)}, bf16[96,2048]{1,0:T(8,128)(2,1)}, u32[]{:S(2)}, u32[]{:S(2)}) collective-permute-start(bf16[96,2048]{1,0:T(8,128)(2,1)S(1)} %pad_maximum_fusion.h0), channel_id=1, source_target_pairs={{0,96},{1,97},{2,98},{3,99},{4,100},{5,101},{6,102},{7,103},{8,104... | collective-permute-start | bytes 1179656 | tf_op jit(solution)/shard_map/ppermute | solution.py:372
  41.4 1.3 %collective-permute-start.3 = (bf16[72,2048]{1,0:T(8,128)(2,1)S(1)}, bf16[72,2048]{1,0:T(8,128)(2,1)S(1)}, u32[]{:S(2)}, u32[]{:S(2)}) collective-permute-start(bf16[72,2048]{1,0:T(8,128)(2,1)S(1)} %pad_maximum_fusion.1), channel_id=1, source_target_pairs={{0,8},{1,9},{2,10},{3,11},{4,12},{5,13},{6,14},{7,15},{8,16},{9,17... | collective-permute-start | bytes 884744 | tf_op jit(solution)/shard_map/ppermute | solution.py:360
  42.7 2.5 %collective-permute-start.4 = (bf16[72,2048]{1,0:T(8,128)(2,1)S(1)}, bf16[72,2048]{1,0:T(8,128)(2,1)S(1)}, u32[]{:S(2)}, u32[]{:S(2)}) collective-permute-start(bf16[72,2048]{1,0:T(8,128)(2,1)S(1)} %pad_maximum_fusion.1), channel_id=1, source_target_pairs={{0,16},{1,17},{2,18},{3,19},{4,20},{5,21},{6,22},{7,23},{8,24},{9,... | collective-permute-start | bytes 884744 | tf_op jit(solution)/shard_map/ppermute | solution.py:360
  45.3 4.8 %worker.1 = bf16[128,2,2048]{2,1,0:T(2,128)(2,1)} custom-call(bf16[128,2,2048]{2,1,0:T(2,128)(2,1)S(1)} %all-to-all-done.arrived_ref, bf16[1,2048,512]{2,1,0:T(8,128)(2,1)} %gate_hbm.1, bf16[1,2048,512]{2,1,0:T(8,128)(2,1)} %up_hbm.1, bf16[1,512,2048]{2,1,0:T(8,128)(2,1)} %down_hbm.1), custom_call_target="tpu_custom_call" | custom-call | flops 3000000000 | bytes 8388608 | tf_op jit(solution)/shard_map/worker/pallas_call | solution.py:216
  50.1 6.4 %all-to-all-start.1 = ((bf16[128,2,2048]{2,1,0:T(2,128)(2,1)}), bf16[128,2,2048]{2,1,0:T(2,128)(2,1)S(1)}, u32[]{:S(2)}, u32[]{:S(2)}) async-start(bf16[128,2,2048]{2,1,0:T(2,128)(2,1)} %worker.1), calls=%async_computation.1 | async-start | bytes 2097152 | tf_op jit(solution)/shard_map/all_to_all | solution.py:407
  58.3 2.1 %collective-permute-start.5 = (bf16[72,2048]{1,0:T(8,128)(2,1)S(1)}, bf16[72,2048]{1,0:T(8,128)(2,1)}, u32[]{:S(2)}, u32[]{:S(2)}) collective-permute-start(bf16[72,2048]{1,0:T(8,128)(2,1)S(1)} %pad_maximum_fusion.1), channel_id=1, source_target_pairs={{0,24},{1,25},{2,26},{3,27},{4,28},{5,29},{6,30},{7,31},{8,0},{9,1... | collective-permute-start | bytes 884744 | tf_op jit(solution)/shard_map/ppermute | solution.py:360
  60.4 15.1 %collective-permute-done.5 = bf16[72,2048]{1,0:T(8,128)(2,1)} collective-permute-done((bf16[72,2048]{1,0:T(8,128)(2,1)S(1)}, bf16[72,2048]{1,0:T(8,128)(2,1)}, u32[]{:S(2)}, u32[]{:S(2)}) %collective-permute-start.5) | collective-permute-done | bytes 294944 | tf_op jit(solution)/shard_map/ppermute | solution.py:360
  75.5 6.0 %concatenate.11.rows_ref = bf16[288,2048]{1,0:T(8,128)(2,1)S(1)} concatenate(bf16[18,2048]{1,0:T(8,128)(2,1)S(1)} %get-tuple-element.22, bf16[18,2048]{1,0:T(8,128)(2,1)S(1)} %collective-permute-done, bf16[18,2048]{1,0:T(8,128)(2,1)S(1)} %collective-permute-done.1, bf16[18,2048]{1,0:T(8,128)(2,1)S(1)} %collective-permute-done.2, bf16[72,2048]{1,0:T(8,128)(2,1)} %copy-done.2, ...), dimensions={0} | concatenate | bytes 2359296 | tf_op jit(solution)/shard_map/concatenate | solution.py:401
  81.6 3.2 %dense.1 = (bf16[72,2176]{1,0:T(8,128)(2,1)S(1)}, bf16[72,2176]{1,0:T(8,128)(2,1)S(1)}, bf16[72,2176]{1,0:T(8,128)(2,1)S(1)}, bf16[72,2176]{1,0:T(8,128)(2,1)S(1)}) custom-call(s32[1]{0:T(128)} %bitcast.8.device_ref, bf16[288,2048]{1,0:T(8,128)(2,1)S(1)} %concatenate.11.rows_ref, bf16[96,2048]{1,0:T(8,128)(2,1)} %copy-done.1, ...), custom_call_target="tpu_custom_call" | custom-call | flops 2000000000 | bytes 6291456 | tf_op jit(solution)/shard_map/dense/pallas_call | solution.py:284
  84.8 2.6 %collective-permute-start.13 = (bf16[72,2176]{1,0:T(8,128)(2,1)S(1)}, bf16[72,2176]{1,0:T(8,128)(2,1)S(1)}, u32[]{:S(2)}, u32[]{:S(2)}) collective-permute-start(bf16[72,2176]{1,0:T(8,128)(2,1)S(1)} %get-tuple-element.24), channel_id=1, source_target_pairs={{0,24},{1,25},{2,26},{3,27},{4,28},{5,29},{6,30},{7,31},{8,0},{9,1... | collective-permute-start | bytes 940040 | tf_op jit(solution)/shard_map/ppermute | solution.py:360
  88.5 5.8 %collective-permute-done.13.b = bf16[72,2176]{1,0:T(8,128)(2,1)S(1)} collective-permute-done((bf16[72,2176]{1,0:T(8,128)(2,1)S(1)}, bf16[72,2176]{1,0:T(8,128)(2,1)S(1)}, u32[]{:S(2)}, u32[]{:S(2)}) %collective-permute-start.13) | collective-permute-done | bytes 313376 | tf_op jit(solution)/shard_map/ppermute | solution.py:360
  94.4 2.9 %collective-permute-done.14.c = bf16[72,2176]{1,0:T(8,128)(2,1)S(1)} collective-permute-done((bf16[72,2176]{1,0:T(8,128)(2,1)S(1)}, bf16[72,2176]{1,0:T(8,128)(2,1)S(1)}, u32[]{:S(2)}, u32[]{:S(2)}) %collective-permute-start.14) | collective-permute-done | bytes 313376 | tf_op jit(solution)/shard_map/ppermute | solution.py:360
  97.2 7.7 %collective-permute-done.15.d = bf16[72,2176]{1,0:T(8,128)(2,1)S(1)} collective-permute-done((bf16[72,2176]{1,0:T(8,128)(2,1)S(1)}, bf16[72,2176]{1,0:T(8,128)(2,1)S(1)}, u32[]{:S(2)}, u32[]{:S(2)}) %collective-permute-start.15) | collective-permute-done | bytes 313376 | tf_op jit(solution)/shard_map/ppermute | solution.py:360
  105.3 1.6 %collective-permute-start.16 = (bf16[18,2176]{1,0:T(8,128)(2,1)S(1)}, bf16[18,2176]{1,0:T(8,128)(2,1)S(1)}, u32[]{:S(2)}, u32[]{:S(2)}) collective-permute-start(bf16[18,2176]{1,0:T(8,128)(2,1)S(1)} %get-tuple-element.28), channel_id=1, source_target_pairs={{0,6},{1,7},{2,0},{3,1},{4,2},{5,3},{6,4},{7,5},{8,14},{9,15},{10,... | collective-permute-start | bytes 235016 | tf_op jit(solution)/shard_map/ppermute | solution.py:360
  109.3 2.6 %collective-permute-done.17.c = bf16[18,2176]{1,0:T(8,128)(2,1)S(1)} collective-permute-done((bf16[18,2176]{1,0:T(8,128)(2,1)S(1)}, bf16[18,2176]{1,0:T(8,128)(2,1)S(1)}, u32[]{:S(2)}, u32[]{:S(2)}) %collective-permute-start.17) | collective-permute-done | bytes 78368 | tf_op jit(solution)/shard_map/ppermute | solution.py:360
  111.9 3.1 %collective-permute-done.18.d = bf16[18,2176]{1,0:T(8,128)(2,1)S(1)} collective-permute-done((bf16[18,2176]{1,0:T(8,128)(2,1)S(1)}, bf16[18,2176]{1,0:T(8,128)(2,1)S(1)}, u32[]{:S(2)}, u32[]{:S(2)}) %collective-permute-start.18) | collective-permute-done | bytes 78368 | tf_op jit(solution)/shard_map/ppermute | solution.py:360
  115.0 1.3 %merger.1 = bf16[18,2048]{1,0:T(8,128)(2,1)} custom-call(bf16[128,2,2048]{2,1,0:T(2,128)(2,1)S(1)} %all-to-all-done.1.returned_ref, f32[256,18]{1,0:T(8,128)S(1)} %get-tuple-element.19.place_ref, bf16[18,2048]{1,0:T(8,128)(2,1)S(1)} %get-tuple-element.20.mixed_ref, f32[18,128]{1,0:T(8,128)S(1)} %get-tuple-element.21.branch_ref, ...), custom_call_target="tpu_custom_call" | custom-call | tf_op jit(solution)/shard_map/merger/pallas_call | solution.py:346
  (40 shorter events, 7.1 us)
Async XLA Ops:
  10.6 16.5 %copy-start.4 = (bf16[32,2048]{1,0:T(8,128)(2,1)S(1)}, bf16[32,2048]{1,0:T(8,128)(2,1)}, u32[]{:S(2)}) copy-start(bf16[32,2048]{1,0:T(8,128)(2,1)} %param.43) | copy-start | bytes 393220
  10.6 34.6 %all-to-all-start = ((bf16[128,2,2048]{2,1,0:T(2,128)(2,1)}), bf16[128,2,2048]{2,1,0:T(2,128)(2,1)S(1)}, u32[]{:S(2)}, u32[]{:S(2)}) async-start(bf16[128,2,2048]{2,1,0:T(2,128)(2,1)} %get-tuple-element.18), calls=%async_computation | async-start | bytes 2097152 | tf_op jit(solution)/shard_map/all_to_all | solution.py:399
  22.1 16.0 %collective-permute-start = (bf16[18,2048]{1,0:T(8,128)(2,1)S(1)}, bf16[18,2048]{1,0:T(8,128)(2,1)S(1)}, u32[]{:S(2)}, u32[]{:S(2)}) collective-permute-start(bf16[18,2048]{1,0:T(8,128)(2,1)S(1)} %get-tuple-element.22), channel_id=1, source_target_pairs={{0,2},{1,3},{2,4},{3,5},{4,6},{5,7},{6,0},{7,1},{8,10},{9,11},{10,... | collective-permute-start | bytes 221192 | tf_op jit(solution)/shard_map/ppermute | solution.py:360
  23.6 17.7 %collective-permute-start.1 = (bf16[18,2048]{1,0:T(8,128)(2,1)S(1)}, bf16[18,2048]{1,0:T(8,128)(2,1)S(1)}, u32[]{:S(2)}, u32[]{:S(2)}) collective-permute-start(bf16[18,2048]{1,0:T(8,128)(2,1)S(1)} %get-tuple-element.22), channel_id=1, source_target_pairs={{0,4},{1,5},{2,6},{3,7},{4,0},{5,1},{6,2},{7,3},{8,12},{9,13},{10,... | collective-permute-start | bytes 221192 | tf_op jit(solution)/shard_map/ppermute | solution.py:360
  26.0 15.3 %collective-permute-start.2 = (bf16[18,2048]{1,0:T(8,128)(2,1)S(1)}, bf16[18,2048]{1,0:T(8,128)(2,1)S(1)}, u32[]{:S(2)}, u32[]{:S(2)}) collective-permute-start(bf16[18,2048]{1,0:T(8,128)(2,1)S(1)} %get-tuple-element.22), channel_id=1, source_target_pairs={{0,6},{1,7},{2,0},{3,1},{4,2},{5,3},{6,4},{7,5},{8,14},{9,15},{10,... | collective-permute-start | bytes 221192 | tf_op jit(solution)/shard_map/ppermute | solution.py:360
  27.2 29.3 %copy-start.1 = (bf16[96,2048]{1,0:T(8,128)(2,1)}, bf16[96,2048]{1,0:T(8,128)(2,1)S(1)}, u32[]{:S(2)}) copy-start(bf16[96,2048]{1,0:T(8,128)(2,1)S(1)} %pad_maximum_fusion.h0) | copy-start | bytes 1179652
  27.2 30.5 %collective-permute-start.7 = (bf16[96,2048]{1,0:T(8,128)(2,1)S(1)}, bf16[96,2048]{1,0:T(8,128)(2,1)}, u32[]{:S(2)}, u32[]{:S(2)}) collective-permute-start(bf16[96,2048]{1,0:T(8,128)(2,1)S(1)} %pad_maximum_fusion.h0), channel_id=1, source_target_pairs={{0,32},{1,33},{2,34},{3,35},{4,36},{5,37},{6,38},{7,39},{8,40},{9,... | collective-permute-start | bytes 1179656 | tf_op jit(solution)/shard_map/ppermute | solution.py:372
  28.6 29.2 %collective-permute-start.9 = (bf16[96,2048]{1,0:T(8,128)(2,1)S(1)}, bf16[96,2048]{1,0:T(8,128)(2,1)}, u32[]{:S(2)}, u32[]{:S(2)}) collective-permute-start(bf16[96,2048]{1,0:T(8,128)(2,1)S(1)} %pad_maximum_fusion.h0), channel_id=1, source_target_pairs={{0,64},{1,65},{2,66},{3,67},{4,68},{5,69},{6,70},{7,71},{8,72},{9,... | collective-permute-start | bytes 1179656 | tf_op jit(solution)/shard_map/ppermute | solution.py:372
  38.2 20.0 %collective-permute-start.11 = (bf16[96,2048]{1,0:T(8,128)(2,1)S(1)}, bf16[96,2048]{1,0:T(8,128)(2,1)}, u32[]{:S(2)}, u32[]{:S(2)}) collective-permute-start(bf16[96,2048]{1,0:T(8,128)(2,1)S(1)} %pad_maximum_fusion.h0), channel_id=1, source_target_pairs={{0,96},{1,97},{2,98},{3,99},{4,100},{5,101},{6,102},{7,103},{8,104... | collective-permute-start | bytes 1179656 | tf_op jit(solution)/shard_map/ppermute | solution.py:372
  41.4 15.1 %collective-permute-start.3 = (bf16[72,2048]{1,0:T(8,128)(2,1)S(1)}, bf16[72,2048]{1,0:T(8,128)(2,1)S(1)}, u32[]{:S(2)}, u32[]{:S(2)}) collective-permute-start(bf16[72,2048]{1,0:T(8,128)(2,1)S(1)} %pad_maximum_fusion.1), channel_id=1, source_target_pairs={{0,8},{1,9},{2,10},{3,11},{4,12},{5,13},{6,14},{7,15},{8,16},{9,17... | collective-permute-start | bytes 884744 | tf_op jit(solution)/shard_map/ppermute | solution.py:360
  42.7 15.6 %collective-permute-start.4 = (bf16[72,2048]{1,0:T(8,128)(2,1)S(1)}, bf16[72,2048]{1,0:T(8,128)(2,1)S(1)}, u32[]{:S(2)}, u32[]{:S(2)}) collective-permute-start(bf16[72,2048]{1,0:T(8,128)(2,1)S(1)} %pad_maximum_fusion.1), channel_id=1, source_target_pairs={{0,16},{1,17},{2,18},{3,19},{4,20},{5,21},{6,22},{7,23},{8,24},{9,... | collective-permute-start | bytes 884744 | tf_op jit(solution)/shard_map/ppermute | solution.py:360
  50.1 31.5 %copy-start = (f32[4096]{0:T(1024)S(1)}, f32[4096]{0:T(1024)}, u32[]{:S(2)}) copy-start(f32[4096]{0:T(1024)} %param.44) | copy-start | bytes 49156
  50.1 64.9 %all-to-all-start.1 = ((bf16[128,2,2048]{2,1,0:T(2,128)(2,1)}), bf16[128,2,2048]{2,1,0:T(2,128)(2,1)S(1)}, u32[]{:S(2)}, u32[]{:S(2)}) async-start(bf16[128,2,2048]{2,1,0:T(2,128)(2,1)} %worker.1), calls=%async_computation.1 | async-start | bytes 2097152 | tf_op jit(solution)/shard_map/all_to_all | solution.py:407
  56.5 25.0 %collective-permute-start.6 = (bf16[96,2048]{1,0:T(8,128)(2,1)S(1)}, bf16[96,2048]{1,0:T(8,128)(2,1)}, u32[]{:S(2)}, u32[]{:S(2)}) collective-permute-start(bf16[96,2048]{1,0:T(8,128)(2,1)S(1)} %pad_maximum_fusion.h0), channel_id=1, source_target_pairs={{0,1},{1,0},{2,3},{3,2},{4,5},{5,4},{6,7},{7,6},{8,9},{9,8},{10,11... | collective-permute-start | bytes 1179656 | tf_op jit(solution)/shard_map/ppermute | solution.py:372
  57.7 23.9 %collective-permute-start.8 = (bf16[96,2048]{1,0:T(8,128)(2,1)}, bf16[96,2048]{1,0:T(8,128)(2,1)}, u32[]{:S(2)}, u32[]{:S(2)}) collective-permute-start(bf16[96,2048]{1,0:T(8,128)(2,1)} %collective-permute-done.7.h2), channel_id=1, source_target_pairs={{0,1},{1,0},{2,3},{3,2},{4,5},{5,4},{6,7},{7,6},{8,9},{9,8},{10,11... | collective-permute-start | bytes 1179656 | tf_op jit(solution)/shard_map/ppermute | solution.py:372
  57.8 23.8 %collective-permute-start.10 = (bf16[96,2048]{1,0:T(8,128)(2,1)}, bf16[96,2048]{1,0:T(8,128)(2,1)}, u32[]{:S(2)}, u32[]{:S(2)}) collective-permute-start(bf16[96,2048]{1,0:T(8,128)(2,1)} %collective-permute-done.9.h4), channel_id=1, source_target_pairs={{0,1},{1,0},{2,3},{3,2},{4,5},{5,4},{6,7},{7,6},{8,9},{9,8},{10,11... | collective-permute-start | bytes 1179656 | tf_op jit(solution)/shard_map/ppermute | solution.py:372
  58.2 23.4 %collective-permute-start.12 = (bf16[96,2048]{1,0:T(8,128)(2,1)}, bf16[96,2048]{1,0:T(8,128)(2,1)}, u32[]{:S(2)}, u32[]{:S(2)}) collective-permute-start(bf16[96,2048]{1,0:T(8,128)(2,1)} %collective-permute-done.11.h6), channel_id=1, source_target_pairs={{0,1},{1,0},{2,3},{3,2},{4,5},{5,4},{6,7},{7,6},{8,9},{9,8},{10,11... | collective-permute-start | bytes 1179656 | tf_op jit(solution)/shard_map/ppermute | solution.py:372
  58.3 17.2 %collective-permute-start.5 = (bf16[72,2048]{1,0:T(8,128)(2,1)S(1)}, bf16[72,2048]{1,0:T(8,128)(2,1)}, u32[]{:S(2)}, u32[]{:S(2)}) collective-permute-start(bf16[72,2048]{1,0:T(8,128)(2,1)S(1)} %pad_maximum_fusion.1), channel_id=1, source_target_pairs={{0,24},{1,25},{2,26},{3,27},{4,28},{5,29},{6,30},{7,31},{8,0},{9,1... | collective-permute-start | bytes 884744 | tf_op jit(solution)/shard_map/ppermute | solution.py:360
  84.8 9.6 %collective-permute-start.13 = (bf16[72,2176]{1,0:T(8,128)(2,1)S(1)}, bf16[72,2176]{1,0:T(8,128)(2,1)S(1)}, u32[]{:S(2)}, u32[]{:S(2)}) collective-permute-start(bf16[72,2176]{1,0:T(8,128)(2,1)S(1)} %get-tuple-element.24), channel_id=1, source_target_pairs={{0,24},{1,25},{2,26},{3,27},{4,28},{5,29},{6,30},{7,31},{8,0},{9,1... | collective-permute-start | bytes 940040 | tf_op jit(solution)/shard_map/ppermute | solution.py:360
  87.4 9.8 %collective-permute-start.14 = (bf16[72,2176]{1,0:T(8,128)(2,1)S(1)}, bf16[72,2176]{1,0:T(8,128)(2,1)S(1)}, u32[]{:S(2)}, u32[]{:S(2)}) collective-permute-start(bf16[72,2176]{1,0:T(8,128)(2,1)S(1)} %get-tuple-element.25), channel_id=1, source_target_pairs={{0,16},{1,17},{2,18},{3,19},{4,20},{5,21},{6,22},{7,23},{8,24},{9,... | collective-permute-start | bytes 940040 | tf_op jit(solution)/shard_map/ppermute | solution.py:360
  88.5 16.4 %collective-permute-start.15 = (bf16[72,2176]{1,0:T(8,128)(2,1)S(1)}, bf16[72,2176]{1,0:T(8,128)(2,1)S(1)}, u32[]{:S(2)}, u32[]{:S(2)}) collective-permute-start(bf16[72,2176]{1,0:T(8,128)(2,1)S(1)} %get-tuple-element.26), channel_id=1, source_target_pairs={{0,8},{1,9},{2,10},{3,11},{4,12},{5,13},{6,14},{7,15},{8,16},{9,17... | collective-permute-start | bytes 940040 | tf_op jit(solution)/shard_map/ppermute | solution.py:360
  105.3 4.1 %collective-permute-start.16 = (bf16[18,2176]{1,0:T(8,128)(2,1)S(1)}, bf16[18,2176]{1,0:T(8,128)(2,1)S(1)}, u32[]{:S(2)}, u32[]{:S(2)}) collective-permute-start(bf16[18,2176]{1,0:T(8,128)(2,1)S(1)} %get-tuple-element.28), channel_id=1, source_target_pairs={{0,6},{1,7},{2,0},{3,1},{4,2},{5,3},{6,4},{7,5},{8,14},{9,15},{10,... | collective-permute-start | bytes 235016 | tf_op jit(solution)/shard_map/ppermute | solution.py:360
  106.8 5.1 %collective-permute-start.17 = (bf16[18,2176]{1,0:T(8,128)(2,1)S(1)}, bf16[18,2176]{1,0:T(8,128)(2,1)S(1)}, u32[]{:S(2)}, u32[]{:S(2)}) collective-permute-start(bf16[18,2176]{1,0:T(8,128)(2,1)S(1)} %get-tuple-element.29), channel_id=1, source_target_pairs={{0,4},{1,5},{2,6},{3,7},{4,0},{5,1},{6,2},{7,3},{8,12},{9,13},{10,... | collective-permute-start | bytes 235016 | tf_op jit(solution)/shard_map/ppermute | solution.py:360
  107.6 7.4 %collective-permute-start.18 = (bf16[18,2176]{1,0:T(8,128)(2,1)S(1)}, bf16[18,2176]{1,0:T(8,128)(2,1)S(1)}, u32[]{:S(2)}, u32[]{:S(2)}) collective-permute-start(bf16[18,2176]{1,0:T(8,128)(2,1)S(1)} %get-tuple-element.30), channel_id=1, source_target_pairs={{0,2},{1,3},{2,4},{3,5},{4,6},{5,7},{6,0},{7,1},{8,10},{9,11},{10,... | collective-permute-start | bytes 235016 | tf_op jit(solution)/shard_map/ppermute | solution.py:360
  (4 other events, 39.1 us)
